TPU v7x, 32 devices: a whole 2x2x4 slice. The times are simulated.
32 devices in a mesh: ep: 32 (over z, y, x, core).
Axes of the slice: x: 2, y: 2, z: 4, core: 2. Of those that a mesh axis runs over, the one named last changes fastest.
Arguments:
- hidden_in: bfloat16 [64, 2048], P('ep'), may hold values from -6 to 6
- lengths: int32 [64], P('ep'), may hold values from 1 to 1024, as said below
- key_cache: bfloat16 [64, 1024, 512], P('ep'), may hold values from -30 to 30
- value_cache: bfloat16 [64, 1024, 512], P('ep'), may hold values from -6 to 6
- query_w: bfloat16 [2048, 2048], P('ep'), may hold values from -0.125 to 0.125
- key_w: bfloat16 [2048, 512], P('ep'), may hold values from -0.125 to 0.125
- value_w: bfloat16 [2048, 512], P('ep'), may hold values from -0.125 to 0.125
- out_w: bfloat16 [2048, 2048], P('ep'), may hold values from -0.125 to 0.125
- lam_heads: float32 [8], replicated, may hold values from 0.3 to 0.8
- head_gain: float32 [256], replicated, may hold values from 0.1 to 1.9
- attn_gain: float32 [2048], replicated, may hold values from 0.1 to 1.9
- moe_gain: float32 [2048], replicated, may hold values from 0.1 to 1.9
- routing: int32 [64, 6], replicated, may hold values from 0 to 31, all different within a row; in each aligned block of 64 rows (0 to 63, 64 to 127, ...) at most 24 rows name the same one
- route_weight: float32 [64, 6], replicated, may hold values from 0.1 to 0.6
- gate_w: bfloat16 [32, 2048, 512], P('ep'), may hold values from -0.125 to 0.125
- up_w: bfloat16 [32, 2048, 512], P('ep'), may hold values from -0.125 to 0.125
- down_w: bfloat16 [32, 512, 2048], P('ep'), may hold values from -0.25 to 0.25
- shared_gate: bfloat16 [2048, 512], replicated, may hold values from -0.125 to 0.125
- shared_up: bfloat16 [2048, 512], replicated, may hold values from -0.125 to 0.125
- shared_down: bfloat16 [512, 2048], replicated, may hold values from -0.25 to 0.25
Outputs:
- layer_out: bfloat16 [64, 2048], P('ep')
- key_new: bfloat16 [64, 512], P('ep')
- value_new: bfloat16 [64, 512], P('ep')
Inputs may be any that keep to these rules, and one draw needn't show every extreme that they name: `lengths`: some sequence has exactly 1024 positions in use. `routing`: each row names 6 different experts; no expert is named by more than 24 rows, a bound that some block reaches.
All inputs are finite; a program needn't handle non-finite values.
Results may differ from a plain program's by a relative error of at most 0.013.
The roundings to bfloat16 on the way count: a program that leaves them out, or rounds other values in their place, can miss the bound.
Values may be sent and summed in bfloat16 or wider, within the bound.
A program may use at most 64 MiB of HBM per device.

v0:
```python
import jax
import jax.numpy as jnp
from jax import lax
from jax.sharding import PartitionSpec as P

KV_HEADS = 2
HEAD_DIM = 128
EXP_CAP = 24


eps_norm = 1e-06
eps_head = 1e-05
theta_base = 500000.0


def rms_scale(row_block, gain_vec, epsilon):
    row_block = row_block.astype(jnp.float32)
    return (
        row_block
        * lax.rsqrt(jnp.mean(row_block * row_block, axis=-1, keepdims=True) + epsilon)
        * gain_vec
    )


def rotate(vectors, positions):
    half_width = vectors.shape[-1] // 2
    inverse = theta_base ** (-jnp.arange(half_width, dtype=jnp.float32) / half_width)
    angles = positions.astype(jnp.float32)[..., None] * inverse
    cosine, sine_part = (jnp.cos(angles), jnp.sin(angles))
    lower_half, upper_half = (vectors[..., :half_width], vectors[..., half_width:])
    return jnp.concatenate(
        [
            lower_half * cosine - upper_half * sine_part,
            lower_half * sine_part + upper_half * cosine,
        ],
        axis=-1,
    )


def attend(queries, key_new, value_new, cache_keys, cache_values, lengths, lam_heads, head_gain):
    num_seqs, kv_heads, group_size = (queries.shape[0], queries.shape[1], queries.shape[2])
    head_dim = queries.shape[-1]
    cache_len = cache_keys.shape[1]
    cache_keys = cache_keys.reshape(num_seqs, cache_len, kv_heads, 2, head_dim)
    cache_values = cache_values.reshape(num_seqs, cache_len, kv_heads, -1)
    value_new = value_new.reshape(num_seqs, kv_heads, -1)
    score_scale = head_dim ** (-0.5)
    scores = (
        jnp.einsum("skgph,sckph->skgpc", queries, cache_keys, preferred_element_type=jnp.float32)
        * score_scale
    )
    self_score = (
        jnp.einsum("skgph,skph->skgp", queries, key_new, preferred_element_type=jnp.float32)
        * score_scale
    )
    live_mask = (jnp.arange(cache_len)[None, :] < lengths[:, None])[:, None, None, None, :]
    peak = jnp.maximum(jnp.max(jnp.where(live_mask, scores, -jnp.inf), axis=-1), self_score)
    weights = jnp.where(live_mask, jnp.exp(scores - peak[..., None]), 0.0)
    self_weight = jnp.exp(self_score - peak)
    totals = jnp.sum(weights, axis=-1) + self_weight
    lambda_grid = lam_heads.reshape(kv_heads, group_size)[None]
    combined = (
        weights[:, :, :, 0] / totals[:, :, :, 0, None]
        - lambda_grid[..., None] * weights[:, :, :, 1] / totals[:, :, :, 1, None]
    ).astype(jnp.bfloat16)
    self_combined = (
        self_weight[..., 0] / totals[..., 0] - lambda_grid * self_weight[..., 1] / totals[..., 1]
    ).astype(jnp.bfloat16)
    head_out = jnp.einsum(
        "skgc,sckv->skgv", combined, cache_values, preferred_element_type=jnp.float32
    )
    head_out = (
        head_out
        + self_combined.astype(jnp.float32)[..., None]
        * value_new.astype(jnp.float32)[:, :, None, :]
    )
    return rms_scale(head_out, head_gain, eps_head).astype(jnp.bfloat16).reshape(num_seqs, -1)


def expert_rows(row_block, routed_here, gate_one, up_one, down_one):
    slot_index = jnp.cumsum(routed_here) - 1
    pick_table = (
        (slot_index[None, :] == jnp.arange(EXP_CAP)[:, None]) & (routed_here[None, :] > 0)
    ).astype(jnp.bfloat16)
    picked = jnp.dot(pick_table, row_block, preferred_element_type=jnp.float32).astype(jnp.bfloat16)
    hidden = (
        jax.nn.silu(jnp.dot(picked, gate_one, preferred_element_type=jnp.float32))
        * jnp.dot(picked, up_one, preferred_element_type=jnp.float32)
    ).astype(jnp.bfloat16)
    result = jnp.dot(hidden, down_one, preferred_element_type=jnp.float32).astype(jnp.bfloat16)
    return jnp.dot(pick_table.T, result, preferred_element_type=jnp.float32)


def on_device(
    hidden_in,
    lengths,
    key_cache,
    value_cache,
    query_w,
    key_w,
    value_w,
    out_w,
    lam_heads,
    head_gain,
    attn_gain,
    moe_gain,
    routing,
    route_weight,
    gate_w,
    up_w,
    down_w,
    shared_gate,
    shared_up,
    shared_down,
):
    device = lax.axis_index("ep")
    tok_dev = hidden_in.shape[0]
    all_rows = lax.all_gather(hidden_in, "ep", axis=0, tiled=True)
    normed = rms_scale(all_rows, attn_gain, eps_norm).astype(jnp.bfloat16)
    joined_rows = jnp.concatenate([query_w, key_w, value_w], axis=1)
    column_block = lax.all_to_all(joined_rows, "ep", split_axis=1, concat_axis=0, tiled=True)
    column_sums = jnp.dot(normed, column_block, preferred_element_type=jnp.float32)
    projected = lax.all_to_all(column_sums, "ep", split_axis=0, concat_axis=1, tiled=True)
    query_cols = query_w.shape[1]
    key_cols = key_w.shape[1]
    queries = rotate(
        projected[:, :query_cols].reshape(tok_dev, KV_HEADS, -1, 2, HEAD_DIM),
        lengths[:, None, None, None],
    ).astype(jnp.bfloat16)
    key_new = rotate(
        projected[:, query_cols : query_cols + key_cols].reshape(tok_dev, KV_HEADS, 2, HEAD_DIM),
        lengths[:, None, None],
    ).astype(jnp.bfloat16)
    value_new = projected[:, query_cols + key_cols :].astype(jnp.bfloat16)
    attn_out = attend(
        queries, key_new, value_new, key_cache, value_cache, lengths, lam_heads, head_gain
    )
    pieces = lax.all_to_all(attn_out, "ep", split_axis=1, concat_axis=0, tiled=True)
    routed_here = jnp.sum((routing == device).astype(jnp.int32), axis=1)
    partial_value = jnp.dot(pieces, out_w, preferred_element_type=jnp.float32)
    attn_proj = lax.psum(partial_value, "ep").astype(jnp.bfloat16)
    mixer_all = (all_rows.astype(jnp.float32) + attn_proj.astype(jnp.float32)).astype(jnp.bfloat16)
    moe_all = rms_scale(mixer_all, moe_gain, eps_norm).astype(jnp.bfloat16)
    weight_col = jnp.sum(jnp.where(routing == device, route_weight, 0.0), axis=1)
    spread_back = (
        expert_rows(moe_all, routed_here, gate_w[0], up_w[0], down_w[0]) * weight_col[:, None]
    )
    routed = lax.psum_scatter(spread_back, "ep", scatter_dimension=0, tiled=True)
    after_mixer = lax.dynamic_slice_in_dim(mixer_all, device * tok_dev, tok_dev, 0)
    moe_in = lax.dynamic_slice_in_dim(moe_all, device * tok_dev, tok_dev, 0)
    shared_hidden = (
        jax.nn.silu(jnp.dot(moe_in, shared_gate, preferred_element_type=jnp.float32))
        * jnp.dot(moe_in, shared_up, preferred_element_type=jnp.float32)
    ).astype(jnp.bfloat16)
    shared_out = jnp.dot(shared_hidden, shared_down, preferred_element_type=jnp.float32)
    layer_out = (after_mixer.astype(jnp.float32) + routed + shared_out).astype(jnp.bfloat16)
    return (layer_out, key_new.reshape(tok_dev, -1), value_new)


def solution(mesh):
    placed = (
        P("ep", None),
        P("ep"),
        P("ep", None, None),
        P("ep", None, None),
        P("ep", None),
        P("ep", None),
        P("ep", None),
        P("ep", None),
        P(),
        P(),
        P(),
        P(),
        P(),
        P(),
        P("ep", None, None),
        P("ep", None, None),
        P("ep", None, None),
        P(),
        P(),
        P(),
    )
    return jax.shard_map(
        on_device,
        mesh=mesh,
        in_specs=placed,
        out_specs=(P("ep", None), P("ep", None), P("ep", None)),
        check_vma=False,
    )
```

profile of v0, /device:TPU:0, one launch (start us, length us, event | category | flops | bytes accessed | tf_op | source)
XLA Modules:
  0.0 275.9 jit_solution(12402558321039086071)
XLA Ops:
  7.2 1.2 pad_maximum_fusion
  8.4 0.5 all_to_all.40
  9.0 1.0 copy.52
  9.9 7.3 %all-to-all-start = ((bf16[64,32,96]{2,0,1:T(8,128)(2,1)}), bf16[64,32,96]{2,0,1:T(8,128)(2,1)S(1)}, u32[]{:S(2)}, u32[]{:S(2)}) async-start(bf16[64,32,96]{2,0,1:T(8,128)(2,1)} %copy.52), calls=%async_computation | async-start | bytes 1048576 | tf_op jit(solution)/shard_map/all_to_all | solution.py:121
  17.5 44.4 %all-gather = bf16[32,2,2048]{2,1,0:T(2,128)(2,1)S(1)} all-gather(bf16[1,2,2048]{2,1,0:T(2,128)(2,1)S(1)} %bitcast.88), channel_id=1, replica_groups=mesh['ep'=32] {'ep'}, dimensions={0}, use_global_device_ids=true | all-gather | bytes 270336 | tf_op jit(solution)/shard_map/all_gather | solution.py:118
  62.0 0.1 multiply_reduce_fusion
  62.1 0.8 multiply_convert_fusion
  62.9 1.1 dot_general.41
  64.4 0.2 fusion.32
  64.6 0.6 copy.55
  65.3 2.6 all-to-all-start.1
  68.0 4.0 %reshape.245 = bf16[2,1024,2,2,128]{4,3,2,1,0:T(2,128)(2,1)} reshape(bf16[2,1024,512]{2,1,0:T(8,128)(2,1)} %param.22) | data formatting | bytes 4194304 | tf_op jit(solution)/shard_map/reshape | solution.py:44
  72.0 3.1 %all-to-all-done.1 = f32[32,2,96]{2,1,0:T(2,128)S(1)} async-done(((f32[32,2,96]{2,1,0:T(2,128)}), f32[32,2,96]{2,1,0:T(2,128)S(1)}, u32[]{:S(2)}, u32[]{:S(2)}) %all-to-all-start.1) | async-done | bytes 24608 | tf_op jit(solution)/shard_map/all_to_all | solution.py:123
  75.6 0.2 fusion.51
  75.8 2.5 select_reduce_fusion
  78.3 0.2 fusion.66
  78.6 0.5 multiply_reduce_fusion.1
  79.3 0.6 copy.62
  79.9 2.7 all-to-all-start.2
  82.8 0.6 convert_element_type.102
  83.4 6.5 %all-to-all-done.2 = bf16[2,32,64]{2,0,1:T(2,128)(2,1)S(1)} async-done(((bf16[2,32,64]{2,0,1:T(2,128)(2,1)}), bf16[2,32,64]{2,0,1:T(2,128)(2,1)S(1)}, u32[]{:S(2)}, u32[]{:S(2)}) %all-to-all-start.2) | async-done | bytes 8224 | tf_op jit(solution)/shard_map/all_to_all | solution.py:138
  89.8 0.2 fusion.68
  90.1 43.0 %all-reduce.5 = bf16[64,2048]{1,0:T(8,128)(2,1)S(1)} all-reduce(f32[64,2048]{1,0:T(8,128)S(1)} %fusion.68), channel_id=1, replica_groups=mesh['ep'=32] {'ep'}, use_global_device_ids=true, to_apply=%region_4.5 | all-reduce | flops 131072 | bytes 786432 | tf_op jit(solution)/shard_map/psum | solution.py:141
  133.0 0.2 fusion.29
  133.2 0.1 fusion.31
  133.4 0.2 convolution_convert_fusion.1
  133.5 2.1 fusion.7
  135.6 0.4 fusion.22
  136.0 1.4 convolution_multiply_fusion
  137.4 2.0 fusion.55
  139.4 126.1 %all-reduce.4.cloned.1.call-done = f32[64,2048]{1,0:T(8,128)} async-done(((f32[64,2048]{1,0:T(8,128)}), f32[64,2048]{1,0:T(8,128)}) %all-reduce.4.cloned.1.call-update) | async-done | bytes 524304
  265.5 3.6 %fusion = bf16[2,2048]{1,0:T(2,128)(2,1)} fusion(bf16[512,2048]{1,0:T(8,128)(2,1)} %param.39, bf16[2048,512]{1,0:T(8,128)(2,1)} %param.38, f32[64,2048]{1,0:T(8,128)} %all-reduce.4.cloned.1.call-done, u32[]{:T(128)S(6)} %multiply.28, bf16[64,2048]{1,0:T(8,128)(2,1)S(1)} %get-tuple-element.6, s32[]{:T(128)S(6)} %select_n.17, f32[2,512]{1,0:T(2,128)S(1)} %fusion.55, ...), kind=kOutput, calls=%fused_computation.4 | convolution fusion | flops 8411136 | bytes 4240896 | tf_op jit(solution)/shard_map/dot_general | solution.py:155
  (62 shorter events, 1.6 us)
Async XLA Ops:
  7.2 128.9 %copy-start = (bf16[1,512,2048]{2,1,0:T(8,128)(2,1)S(1)}, bf16[1,512,2048]{2,1,0:T(8,128)(2,1)}, u32[]{:S(2)}) copy-start(bf16[1,512,2048]{2,1,0:T(8,128)(2,1)} %param.36) | copy-start | bytes 6291460
  7.2 10.1 %copy-start.10 = (s32[2]{0:T(128)S(1)}, s32[2]{0:T(128)}, u32[]{:S(2)}) copy-start(s32[2]{0:T(128)} %param.21) | copy-start | bytes 28
  7.2 10.1 %copy-start.7 = (f32[64,6]{0,1:T(8,128)S(1)}, f32[64,6]{0,1:T(8,128)}, u32[]{:S(2)}) copy-start(f32[64,6]{0,1:T(8,128)} %param.33) | copy-start | bytes 4612
  7.2 10.1 %copy-start.8 = (s32[64,6]{0,1:T(8,128)S(1)}, s32[64,6]{0,1:T(8,128)}, u32[]{:S(2)}) copy-start(s32[64,6]{0,1:T(8,128)} %param.32) | copy-start | bytes 4612
  7.2 10.3 %copy-start.5 = (bf16[2,2048]{1,0:T(2,128)(2,1)S(1)}, bf16[2,2048]{1,0:T(2,128)(2,1)}, u32[]{:S(2)}) copy-start(bf16[2,2048]{1,0:T(2,128)(2,1)} %param.20) | copy-start | bytes 24580
  8.9 53.2 %copy-start.3 = (f32[2048]{0:T(1024)S(1)}, f32[2048]{0:T(1024)}, u32[]{:S(2)}) copy-start(f32[2048]{0:T(1024)} %param.30) | copy-start | bytes 24580
  9.9 54.4 %all-to-all-start = ((bf16[64,32,96]{2,0,1:T(8,128)(2,1)}), bf16[64,32,96]{2,0,1:T(8,128)(2,1)S(1)}, u32[]{:S(2)}, u32[]{:S(2)}) async-start(bf16[64,32,96]{2,0,1:T(8,128)(2,1)} %copy.52), calls=%async_computation | async-start | bytes 1048576 | tf_op jit(solution)/shard_map/all_to_all | solution.py:121
  17.3 50.7 %copy-start.12 = (f32[8]{0:T(128)S(1)}, f32[8]{0:T(128)}, u32[]{:S(2)}) copy-start(f32[8]{0:T(128)} %param.28) | copy-start | bytes 100
  65.3 9.8 %all-to-all-start.1 = ((f32[32,2,96]{2,1,0:T(2,128)}), f32[32,2,96]{2,1,0:T(2,128)S(1)}, u32[]{:S(2)}, u32[]{:S(2)}) async-start(f32[32,2,96]{2,1,0:T(2,128)} %copy.55), calls=%async_computation.1 | async-start | bytes 65536 | tf_op jit(solution)/shard_map/all_to_all | solution.py:123
  75.2 3.9 %copy-start.6 = (bf16[2,512]{1,0:T(2,128)(2,1)}, bf16[2,512]{1,0:T(2,128)(2,1)S(1)}, u32[]{:S(2)}) copy-start(bf16[2,512]{1,0:T(2,128)(2,1)S(1)} %slice.101) | copy-start | bytes 6148
  75.3 3.3 %copy-start.11 = (bf16[2,1024,512]{2,1,0:T(8,128)(2,1)S(1)}, bf16[2,1024,512]{2,1,0:T(8,128)(2,1)}, u32[]{:S(2)}) copy-start(bf16[2,1024,512]{2,1,0:T(8,128)(2,1)} %param.23) | copy-start | bytes 6291460
  78.3 0.8 copy-start.9
  78.3 11.6 %copy-start.2 = (bf16[64,2048]{1,0:T(8,128)(2,1)S(1)}, bf16[64,2048]{1,0:T(8,128)(2,1)}, u32[]{:S(2)}) copy-start(bf16[64,2048]{1,0:T(8,128)(2,1)} %param.27) | copy-start | bytes 786436
  79.1 54.1 %copy-start.4 = (f32[2048]{0:T(1024)S(1)}, f32[2048]{0:T(1024)}, u32[]{:S(2)}) copy-start(f32[2048]{0:T(1024)} %param.31) | copy-start | bytes 24580
  79.9 9.9 %all-to-all-start.2 = ((bf16[2,32,64]{2,0,1:T(2,128)(2,1)}), bf16[2,32,64]{2,0,1:T(2,128)(2,1)S(1)}, u32[]{:S(2)}, u32[]{:S(2)}) async-start(bf16[2,32,64]{2,0,1:T(2,128)(2,1)} %copy.62), calls=%async_computation.2 | async-start | bytes 32768 | tf_op jit(solution)/shard_map/all_to_all | solution.py:138
  82.7 182.9 %all-reduce.4.cloned.1.call-start = ((), (), s32[]{:S(2)}) async-start(), calls=%async_computation.3 | async-start | bytes 1048576
  133.0 2.6 copy-start.1
Sparse Core Ops, SparseCore 0:
  137.5 127.9 all-reduce.3
where the time goes:
time: 276 us
  waiting for transfers between devices  136 us (49%)
  blocking collectives  87.4 us (32%)
  between operations  14.4 us (5%)
  matrix products  13.2 us (5%)
  starting transfers between devices  12.7 us (5%)
  local copies, waits for them, and re-layouts  9.12 us (3%)
  other arithmetic  3.5 us (1%)
    unnamed x2, waiting for transfers between devices  126 us
    all_gather x1, blocking collectives, on_device(): all_rows = lax.all_gather(hidden_in, 'ep', axis=0, tiled=True)  44.4 us
    psum x1, blocking collectives, on_device(): attn_proj = lax.psum(partial_value, 'ep').astype(jnp.bfloat16)  43 us
    all_to_all x1, starting transfers between devices, on_device(): lax.all_to_all(joined_rows, 'ep', split_axis=1, concat_axis=0, tiled=True)  7.33 us
    all_to_all x1, waiting for transfers between devices, on_device(): lax.all_to_all(attn_out, 'ep', split_axis=1, concat_axis=0, tiled=True)  6.46 us
  transfers between devices with their start and end apart: 4, of which 3 were waited for; matrix products, arithmetic and copies ran while one was open for 3% of the time, Pallas kernels for 0%

commit v1 on v0

v1 whole, which is shorter than its diff:
```python
import functools

import jax
import jax.numpy as jnp
import numpy as np
from jax import lax
from jax.experimental import pallas as pl
from jax.experimental.pallas import tpu as pltpu
from jax.sharding import PartitionSpec as P

KV_HEADS = 2
HEAD_DIM = 128
LANES = 128

eps_norm = 1e-06
eps_head = 1e-05
theta_base = 500000.0

MESH = pl.DeviceIdType.MESH
f32 = jnp.float32
bf16 = jnp.bfloat16


def inv_rms(rows, epsilon):
    return lax.rsqrt(jnp.mean(rows * rows, axis=-1, keepdims=True) + epsilon)


def wait_bytes(ref, sem):
    pltpu.make_async_copy(ref, ref, sem).wait()


def layer_kernel(
    n,
    lengths,
    lam,
    hidden_hbm,
    keys_hbm,
    values_hbm,
    qw_hbm,
    kw_hbm,
    vw_hbm,
    ow_hbm,
    gate_hbm,
    up_hbm,
    down_hbm,
    sgate_hbm,
    sup_hbm,
    sdown_hbm,
    head_gain,
    attn_gain,
    moe_gain,
    routing,
    route_weight,
    freqs,
    out_ref,
    key_out,
    value_out,
    hid,
    w_in,
    w_out,
    keys,
    values,
    gate,
    up,
    down,
    sgate,
    sup,
    sdown,
    gat,
    wq,
    wo,
    rows32,
    rows16,
    csum,
    proj,
    abuf,
    att,
    obuf,
    cols,
    hbuf,
    res,
    ebuf,
    back,
    local_sem,
    send_sem,
    recv_sem,
    tile_sem,
):
    me = lax.axis_index("ep")
    tok, width = hid.shape
    rows = w_in.shape[0]
    in_tiles, out_tiles = proj.shape[0], cols.shape[0]
    q_tiles = qw_hbm.shape[1] // LANES
    k_tiles = kw_hbm.shape[1] // LANES
    group = q_tiles // (2 * KV_HEADS)
    total = n * tok
    peers_step = 16 // tok

    def load(src, dst, i):
        copy = pltpu.make_async_copy(src, dst, local_sem.at[i])
        copy.start()
        return copy

    def put(src, dst, phase, target, sent=None):
        pltpu.make_async_remote_copy(
            src_ref=src,
            dst_ref=dst,
            send_sem=send_sem.at[phase] if sent is None else sent,
            recv_sem=recv_sem.at[phase],
            device_id=(target,),
            device_id_type=MESH,
        ).start()

    def keep(src, dst, phase):
        pltpu.make_async_copy(src, dst, recv_sem.at[phase]).start()

    def put_or_keep(src, dst, phase, target):
        @pl.when(target != me)
        def _():
            put(src, dst, phase, target)

        @pl.when(target == me)
        def _():
            keep(src, dst, phase)

    def each_peer(body):
        def step(k, carry):
            body(lax.rem(me + k, n))
            return carry

        lax.fori_loop(1, n, step, 0)

    q_width, k_width = qw_hbm.shape[1], kw_hbm.shape[1]
    first = [
        load(hidden_hbm, hid, 0),
        load(qw_hbm, w_in.at[:, pl.ds(0, q_width)], 1),
        load(kw_hbm, w_in.at[:, pl.ds(q_width, k_width)], 2),
        load(vw_hbm, w_in.at[:, pl.ds(q_width + k_width, vw_hbm.shape[1])], 3),
        load(ow_hbm, w_out, 4),
    ]
    barrier = pltpu.get_barrier_semaphore()
    each_peer(
        lambda p: pl.semaphore_signal(barrier, inc=1, device_id=(p,), device_id_type=MESH)
    )
    load_keys = load(keys_hbm, keys, 5)
    load_values = load(values_hbm, values, 6)
    load_gate = load(gate_hbm.at[0], gate, 7)
    load_up = load(up_hbm.at[0], up, 8)
    load_down = load(down_hbm.at[0], down, 9)
    load_sgate = load(sgate_hbm, sgate, 10)
    load_sup = load(sup_hbm, sup, 11)
    load_sdown = load(sdown_hbm, sdown, 12)
    for copy in first:
        copy.wait()
    pl.semaphore_wait(barrier, n - 1)

    each_peer(lambda p: put(hid, gat.at[me], 0, p))
    keep(hid, gat.at[me], 0)
    own_rows = pl.ds(pl.multiple_of(me * rows, rows), rows)
    in_owner = lambda c: (c * n) // in_tiles
    stride = n // out_tiles
    out_owner = lambda c: c * stride + stride - 1

    def send_in(k, carry):
        c = lax.rem(k + me, in_tiles)
        cols_c = pl.ds(pl.multiple_of(c * LANES, LANES), LANES)
        put_or_keep(w_in.at[:, cols_c], wq.at[own_rows, :], 1, in_owner(c))
        return carry

    lax.fori_loop(0, in_tiles, send_in, 0)

    def send_out(k, carry):
        c = lax.rem(k + me, out_tiles)
        cols_c = pl.ds(pl.multiple_of(c * LANES, LANES), LANES)
        put_or_keep(w_out.at[:, cols_c], wo.at[own_rows, :], 2, out_owner(c))
        return carry

    lax.fori_loop(0, out_tiles, send_out, 0)
    my_in = (me * in_tiles + n - 1) // n
    has_in = in_owner(my_in) == me
    my_out = me // stride
    has_out = lax.rem(me, stride) == stride - 1

    def stacked(buf, i):
        return jnp.concatenate(
            [buf[i * peers_step + k].astype(f32) for k in range(peers_step)], axis=0
        )

    wait_bytes(gat, recv_sem.at[0])

    def norm_rows(i, carry):
        x = stacked(gat, i)
        at = pl.ds(pl.multiple_of(i * 16, 16), 16)
        rows32[at, :] = x
        rows16[at, :] = (x * inv_rms(x, eps_norm) * attn_gain[...]).astype(bf16)
        return carry

    lax.fori_loop(0, total // 16, norm_rows, 0)

    @pl.when(has_in)
    def _():
        wait_bytes(wq, recv_sem.at[1])
        sums = jnp.dot(rows16[...], wq[...], preferred_element_type=f32)
        for p in range(n):
            csum[p] = sums[p * tok : (p + 1) * tok, :]
        each_peer(lambda p: put(csum.at[p], proj.at[my_in], 3, p))
        keep(csum.at[me], proj.at[my_in], 3)

    row_id = lax.broadcasted_iota(jnp.int32, (tok, LANES), 0)
    position = jnp.zeros((tok, LANES), jnp.int32)
    for s in range(tok):
        position = jnp.where(row_id == s, lengths[s], position)
    angle = position.astype(f32) * freqs[...]
    cosine, sine = jnp.cos(angle), jnp.sin(angle)
    low = lax.broadcasted_iota(jnp.int32, (tok, LANES), 1) < LANES // 2
    sine = jnp.where(low, -sine, sine)
    load_keys.wait()
    load_values.wait()
    wait_bytes(proj, recv_sem.at[3])
    turned = []
    for c in range(q_tiles + k_tiles):
        x = proj[c]
        turned.append((x * cosine + pltpu.roll(x, LANES // 2, 1) * sine).astype(bf16).astype(f32))
    new_values = [proj[c].astype(bf16).astype(f32) for c in range(q_tiles + k_tiles, in_tiles)]
    key_out[...] = jnp.concatenate(turned[q_tiles:], axis=1).astype(bf16)
    value_out[...] = jnp.concatenate(new_values, axis=1).astype(bf16)
    v_tiles = len(new_values) // KV_HEADS

    cache_len = keys.shape[1]
    scale = HEAD_DIM ** (-0.5)
    pairs = 2 * group
    value_dim = v_tiles * LANES
    first_map = lax.broadcasted_iota(jnp.int32, (pairs, cache_len), 0) < group
    spot = lax.broadcasted_iota(jnp.int32, (pairs, cache_len), 1)
    contract = (((1,), (1,)), ((), ()))
    out_rows = []
    for s in range(tok):
        heads = []
        for kv in range(KV_HEADS):
            q = jnp.concatenate(
                [
                    turned[(kv * group + g) * 2 + j][s : s + 1]
                    for j in range(2)
                    for g in range(group)
                ],
                axis=0,
            )
            own_key = jnp.concatenate(
                [turned[q_tiles + kv * 2 + j][s : s + 1] for j in range(2) for g in range(group)],
                axis=0,
            )
            q16 = q.astype(bf16)
            parts = [
                lax.dot_general(
                    q16,
                    keys[s, :, (kv * 2 + j) * LANES : (kv * 2 + j + 1) * LANES],
                    contract,
                    preferred_element_type=f32,
                )
                for j in range(2)
            ]
            live = spot < lengths[s]
            scores = jnp.where(live, jnp.where(first_map, parts[0], parts[1]) * scale, -jnp.inf)
            self_score = jnp.sum(q * own_key, axis=1, keepdims=True) * scale
            peak = jnp.maximum(jnp.max(scores, axis=1, keepdims=True), self_score)
            weights = jnp.exp(scores - peak)
            self_weight = jnp.exp(self_score - peak)
            totals = jnp.sum(weights, axis=1, keepdims=True) + self_weight
            map_row = lax.broadcasted_iota(jnp.int32, (pairs, 1), 0)
            factor = jnp.ones((pairs, 1), f32)
            for g in range(group):
                factor = jnp.where(map_row == group + g, lam[kv * group + g], factor)
            factor = factor / totals
            scaled = weights * factor
            self_scaled = jnp.broadcast_to(self_weight * factor, (pairs, LANES))
            combined = (scaled[:group] - scaled[group:]).astype(bf16)
            self_comb = (self_scaled[:group] - self_scaled[group:]).astype(bf16).astype(f32)
            head = jnp.dot(
                combined,
                values[s, :, kv * value_dim : (kv + 1) * value_dim],
                preferred_element_type=f32,
            )
            own_value = jnp.concatenate(
                [new_values[kv * v_tiles + v][s : s + 1] for v in range(v_tiles)], axis=1
            )
            head = head + self_comb[:, :1] * own_value
            head = head * inv_rms(head, eps_head) * head_gain[...]
            heads += [head[g : g + 1] for g in range(group)]
        out_rows.append(jnp.concatenate(heads, axis=1))
    abuf[...] = jnp.concatenate(out_rows, axis=0).astype(bf16)

    def send_att(k, carry):
        put_or_keep(abuf, att.at[me], 4, out_owner(lax.rem(k + my_out, out_tiles)))
        return carry

    lax.fori_loop(0, out_tiles, send_att, 0)

    @pl.when(has_out)
    def _():
        wait_bytes(wo, recv_sem.at[2])
        wait_bytes(att, recv_sem.at[4])

        def stack_rows(i, carry):
            rows16[pl.ds(pl.multiple_of(i * 16, 16), 16), :] = stacked(att, i).astype(bf16)
            return carry

        lax.fori_loop(0, total // 16, stack_rows, 0)
        obuf[...] = jnp.dot(rows16[...], wo[...], preferred_element_type=f32).astype(bf16)
        each_peer(lambda p: put(obuf, cols.at[my_out], 5, p, tile_sem.at[p]))
        keep(obuf, cols.at[my_out], 5)

    wait_bytes(cols, recv_sem.at[5])

    def mix_rows(i, carry):
        at = pl.ds(pl.multiple_of(i * 16, 16), 16)
        added = jnp.concatenate([cols[c, at, :] for c in range(out_tiles)], axis=1)
        x = (rows32[at, :] + added.astype(f32)).astype(bf16).astype(f32)
        rows32[at, :] = x
        rows16[at, :] = (x * inv_rms(x, eps_norm) * moe_gain[...]).astype(bf16)
        return carry

    lax.fori_loop(0, total // 16, mix_rows, 0)
    load_gate.wait()
    load_up.wait()
    load_down.wait()

    def hide(block, gate_w, up_w, at):
        g = jnp.dot(block, gate_w[:, at], preferred_element_type=f32)
        u = jnp.dot(block, up_w[:, at], preferred_element_type=f32)
        return (g * jax.nn.sigmoid(g) * u).astype(bf16)

    chunk = 256
    for c in range(gate.shape[1] // chunk):
        at = slice(c * chunk, (c + 1) * chunk)
        hbuf[:, at] = hide(rows16[...], gate, up, at)
    for c in range(width // chunk):
        at = slice(c * chunk, (c + 1) * chunk)
        res[:, at] = jnp.dot(hbuf[...], down[:, at], preferred_element_type=f32)

    def split_rows(i, carry):
        block = res[pl.ds(pl.multiple_of(i * 16, 16), 16), :]
        for k in range(peers_step):
            ebuf[i * peers_step + k] = block[k * tok : (k + 1) * tok, :].astype(bf16)
        return carry

    lax.fori_loop(0, total // 16, split_rows, 0)
    each_peer(lambda p: put(ebuf.at[p], back.at[me], 6, p))
    keep(ebuf.at[me], back.at[me], 6)

    load_sgate.wait()
    load_sup.wait()
    load_sdown.wait()
    per_block = 8 // tok

    def own(ref):
        block = ref[pl.ds(pl.multiple_of(me // per_block * 8, 8), 8), :]
        picked = block[:tok]
        for k in range(1, per_block):
            here = lax.rem(me, per_block) == k
            picked = jnp.where(here, block[k * tok : (k + 1) * tok], picked)
        return picked

    after_mixer = own(rows32)
    moe_in = (after_mixer * inv_rms(after_mixer, eps_norm) * moe_gain[...]).astype(bf16)
    shared_hidden = jnp.concatenate(
        [
            hide(moe_in, sgate, sup, slice(c * chunk, (c + 1) * chunk))
            for c in range(sgate.shape[1] // chunk)
        ],
        axis=1,
    )
    shared_out = jnp.concatenate(
        [
            jnp.dot(
                shared_hidden,
                sdown[:, c * chunk : (c + 1) * chunk],
                preferred_element_type=f32,
            )
            for c in range(width // chunk)
        ],
        axis=1,
    )
    named = own(routing)
    named_weight = own(route_weight)
    expert_id = lax.broadcasted_iota(jnp.int32, (tok, n), 1)
    table = jnp.zeros((tok, n), f32)
    for k in range(named.shape[1]):
        table = table + jnp.where(
            expert_id == named[:, k : k + 1], named_weight[:, k : k + 1], 0.0
        )
    wait_bytes(back, recv_sem.at[6])
    routed = jnp.zeros((tok, width), f32)
    for e in range(n):
        routed = routed + table[:, e : e + 1] * back[e].astype(f32)
    out_ref[...] = (after_mixer + routed + shared_out).astype(bf16)

    others = pl.ds(0, n - 1)
    wait_bytes(gat.at[others], send_sem.at[0])
    wait_bytes(back.at[others], send_sem.at[6])

    def drain(mine, some, every, phase):
        @pl.when(mine)
        def _():
            wait_bytes(some, send_sem.at[phase])

        @pl.when(jnp.logical_not(mine))
        def _():
            wait_bytes(every, send_sem.at[phase])

    drain(has_in, w_in.at[:, pl.ds(0, (in_tiles - 1) * LANES)], w_in, 1)
    drain(has_out, w_out.at[:, pl.ds(0, (out_tiles - 1) * LANES)], w_out, 2)
    drain(has_out, att.at[pl.ds(0, out_tiles - 1)], att.at[pl.ds(0, out_tiles)], 4)

    @pl.when(has_in)
    def _():
        wait_bytes(csum.at[others], send_sem.at[3])

    @pl.when(has_out)
    def _():
        each_peer(lambda p: wait_bytes(obuf, tile_sem.at[p]))


def on_device(
    n,
    hidden_in,
    lengths,
    key_cache,
    value_cache,
    query_w,
    key_w,
    value_w,
    out_w,
    lam_heads,
    head_gain,
    attn_gain,
    moe_gain,
    routing,
    route_weight,
    gate_w,
    up_w,
    down_w,
    shared_gate,
    shared_up,
    shared_down,
):
    tok, width = hidden_in.shape
    total = n * tok
    rows = query_w.shape[0]
    in_width = query_w.shape[1] + key_w.shape[1] + value_w.shape[1]
    in_tiles, out_tiles = in_width // LANES, width // LANES
    half = HEAD_DIM // 2
    inverse = np.power(theta_base, -np.arange(half) / half).astype(np.float32)
    freqs = jnp.asarray(np.concatenate([inverse, inverse])[None, :])
    smem = pl.BlockSpec(memory_space=pltpu.SMEM)
    vmem = pl.BlockSpec(memory_space=pltpu.VMEM)
    hbm = pl.BlockSpec(memory_space=pl.ANY)
    like = lambda a: pltpu.VMEM(a.shape, a.dtype)
    return pl.pallas_call(
        functools.partial(layer_kernel, n),
        out_shape=(
            jax.ShapeDtypeStruct((tok, width), bf16),
            jax.ShapeDtypeStruct((tok, key_w.shape[1]), bf16),
            jax.ShapeDtypeStruct((tok, value_w.shape[1]), bf16),
        ),
        in_specs=[smem] * 2 + [hbm] * 13 + [vmem] * 6,
        out_specs=(vmem, vmem, vmem),
        scratch_shapes=[
            like(hidden_in),
            pltpu.VMEM((rows, in_width), bf16),
            like(out_w),
            like(key_cache),
            like(value_cache),
            pltpu.VMEM(gate_w.shape[1:], bf16),
            pltpu.VMEM(up_w.shape[1:], bf16),
            pltpu.VMEM(down_w.shape[1:], bf16),
            like(shared_gate),
            like(shared_up),
            like(shared_down),
            pltpu.VMEM((n, tok, width), bf16),
            pltpu.VMEM((n * rows, LANES), bf16),
            pltpu.VMEM((n * out_w.shape[0], LANES), bf16),
            pltpu.VMEM((total, width), f32),
            pltpu.VMEM((total, width), bf16),
            pltpu.VMEM((n, tok, LANES), f32),
            pltpu.VMEM((in_tiles, tok, LANES), f32),
            pltpu.VMEM((tok, width), bf16),
            pltpu.VMEM((n, tok, width), bf16),
            pltpu.VMEM((total, LANES), bf16),
            pltpu.VMEM((out_tiles, total, LANES), bf16),
            pltpu.VMEM((total, gate_w.shape[2]), bf16),
            pltpu.VMEM((total, width), f32),
            pltpu.VMEM((n, tok, width), bf16),
            pltpu.VMEM((n, tok, width), bf16),
            pltpu.SemaphoreType.DMA((13,)),
            pltpu.SemaphoreType.DMA((7,)),
            pltpu.SemaphoreType.DMA((7,)),
            pltpu.SemaphoreType.DMA((n,)),
        ],
        compiler_params=pltpu.CompilerParams(
            collective_id=0, has_side_effects=True, vmem_limit_bytes=64000000
        ),
        name="decode_layer",
    )(
        lengths,
        lam_heads,
        hidden_in,
        key_cache,
        value_cache,
        query_w,
        key_w,
        value_w,
        out_w,
        gate_w,
        up_w,
        down_w,
        shared_gate,
        shared_up,
        shared_down,
        head_gain[None, :],
        attn_gain[None, :],
        moe_gain[None, :],
        routing,
        route_weight,
        freqs,
    )


def solution(mesh):
    placed = (
        P("ep", None),
        P("ep"),
        P("ep", None, None),
        P("ep", None, None),
        P("ep", None),
        P("ep", None),
        P("ep", None),
        P("ep", None),
        P(),
        P(),
        P(),
        P(),
        P(),
        P(),
        P("ep", None, None),
        P("ep", None, None),
        P("ep", None, None),
        P(),
        P(),
        P(),
    )
    return jax.shard_map(
        functools.partial(on_device, mesh.shape["ep"]),
        mesh=mesh,
        in_specs=placed,
        out_specs=(P("ep", None), P("ep", None), P("ep", None)),
        check_vma=False,
    )
```

time: 276 us -> 65 us (0.24)
  waiting for transfers between devices: 136 us -> 0 us
  blocking collectives: 87.4 us -> 0 us
  Pallas kernels: 0 us -> 56.4 us
  between operations: 14.4 us -> 0.64 us
  matrix products: 13.2 us -> 0 us
  starting transfers between devices: 12.7 us -> 0 us
  other arithmetic: 3.5 us -> 0 us
    unnamed x2 -> x0, waiting for transfers between devices: 126 us -> none
    pallas_call x0 -> x1, Pallas kernels: none -> 56.4 us  [on_device(): pl.pallas_call(functools.partial(layer_kernel, n), out_shape=(jax.ShapeDt...]
    all_gather x1 -> x0, blocking collectives: 44.4 us -> none  [on_device(): all_rows = lax.all_gather(hidden_in, 'ep', axis=0, tiled=True)]
    psum x1 -> x0, blocking collectives: 43 us -> none  [on_device(): attn_proj = lax.psum(partial_value, 'ep').astype(jnp.bfloat16)]
    dot_general x11 -> x0, matrix products: 13.2 us -> none  [the longest x1 3.56 us: on_device(): jnp.dot(shared_hidden, shared_down, preferred_element_type=jnp.float32)]
    all_to_all x3 -> x0, starting transfers between devices: 12.6 us -> none  [the longest x1 7.33 us: on_device(): lax.all_to_all(joined_rows, 'ep', split_axis=1, concat_axis=0, tiled=True)]
    all_to_all x3 -> x0, waiting for transfers between devices: 9.55 us -> none  [the longest x1 6.46 us: on_device(): lax.all_to_all(attn_out, 'ep', split_axis=1, concat_axis=0, tiled=True)]
    unnamed x26 -> x5, local copies, waits for them, and re-layouts: 0.07 us -> 6.61 us
  transfers between devices with their start and end apart: 4 -> 0, of which waited for: 3 -> 0; matrix products, arithmetic and copies ran while one was open for 3% -> 0% of each run, Pallas kernels for 0% -> 0%
where the time goes in v1:
time: 65 us; the launch traced here: 63.7 us
  Pallas kernels  56.4 us (87%)
  local copies, waits for them, and re-layouts  6.61 us (10%)
    pallas_call x1, Pallas kernels, on_device(): pl.pallas_call(functools.partial(layer_kernel, n), out_shape=(jax.ShapeDt...  56.4 us
    unnamed x5, local copies, waits for them, and re-layouts  6.61 us

profile of v1, /device:TPU:0, one launch (start us, length us, event | category | flops | bytes accessed | tf_op | source)
XLA Modules:
  0.0 63.7 jit_solution(15592932122036063657)
XLA Ops:
  0.6 1.4 %copy.24.routing = s32[64,6]{1,0:T(8,128)} copy(s32[64,6]{0,1:T(8,128)} %param.33) | data formatting | bytes 3072 | tf_op args[12]
  2.0 1.4 %copy.25.route_weight = f32[64,6]{1,0:T(8,128)} copy(f32[64,6]{0,1:T(8,128)} %param.34) | data formatting | bytes 3072 | tf_op args[13]
  3.4 56.4 %decode_layer.1 = (bf16[2,2048]{1,0:T(2,128)(2,1)}, bf16[2,512]{1,0:T(2,128)(2,1)}, bf16[2,512]{1,0:T(2,128)(2,1)}) custom-call(s32[2]{0:T(128)} %lengths.1, f32[8]{0:T(128)} %lam.1, bf16[2,2048]{1,0:T(2,128)(2,1)} %hidden_hbm.1, bf16[2,1024,512]{2,1,0:T(8,128)(2,1)} %keys_hbm.1, bf16[2,1024,512]{2,1,0:T(8,128)(2,1)} %values_hbm.1, bf16[64,2048]{1,0:T(8,128)(2,1)} %qw_hbm.1, ...), custom_call_target="tpu_custom_call" | custom-call | tf_op jit(solution)/shard_map/decode_layer/pallas_call | solution.py:458
  59.9 1.3 %copy.29 = bf16[2,2048]{1,0:T(2,128)(2,1)} copy(bf16[2,2048]{1,0:T(2,128)(2,1)} %get-tuple-element.6) | data formatting | bytes 16384
  61.2 1.3 %copy.30 = bf16[2,512]{1,0:T(2,128)(2,1)} copy(bf16[2,512]{1,0:T(2,128)(2,1)} %get-tuple-element.7) | data formatting | bytes 4096
  62.4 1.3 %copy.31 = bf16[2,512]{1,0:T(2,128)(2,1)} copy(bf16[2,512]{1,0:T(2,128)(2,1)} %get-tuple-element.8) | data formatting | bytes 4096

commit v2 on v1

--- a/solution.py
+++ b/solution.py
@@ -1,4 +1,5 @@
 import functools
+import math
 
 import jax
 import jax.numpy as jnp
@@ -66,17 +67,20 @@
     sgate,
     sup,
     sdown,
-    gat,
+    nbuf,
+    xin,
     wq,
     wo,
-    rows32,
-    rows16,
+    xrows,
     csum,
     proj,
     abuf,
     att,
-    obuf,
-    cols,
+    osum,
+    oproj,
+    mbuf,
+    gat,
+    rows16,
     hbuf,
     res,
     ebuf,
@@ -84,12 +88,15 @@
     local_sem,
     send_sem,
     recv_sem,
-    tile_sem,
 ):
     me = lax.axis_index("ep")
     tok, width = hid.shape
     rows = w_in.shape[0]
-    in_tiles, out_tiles = proj.shape[0], cols.shape[0]
+    in_block, out_block = wq.shape[1], wo.shape[1]
+    depth = wq.shape[0]
+    size = depth // rows
+    blocks = n // size
+    in_tiles = size * in_block // LANES
     q_tiles = qw_hbm.shape[1] // LANES
     k_tiles = kw_hbm.shape[1] // LANES
     group = q_tiles // (2 * KV_HEADS)
@@ -101,11 +108,11 @@
         copy.start()
         return copy
 
-    def put(src, dst, phase, target, sent=None):
+    def put(src, dst, phase, target):
         pltpu.make_async_remote_copy(
             src_ref=src,
             dst_ref=dst,
-            send_sem=send_sem.at[phase] if sent is None else sent,
+            send_sem=send_sem.at[phase],
             recv_sem=recv_sem.at[phase],
             device_id=(target,),
             device_id_type=MESH,
@@ -113,15 +120,6 @@
 
     def keep(src, dst, phase):
         pltpu.make_async_copy(src, dst, recv_sem.at[phase]).start()
-
-    def put_or_keep(src, dst, phase, target):
-        @pl.when(target != me)
-        def _():
-            put(src, dst, phase, target)
-
-        @pl.when(target == me)
-        def _():
-            keep(src, dst, phase)
 
     def each_peer(body):
         def step(k, carry):
@@ -150,61 +148,58 @@
     load_sgate = load(sgate_hbm, sgate, 10)
     load_sup = load(sup_hbm, sup, 11)
     load_sdown = load(sdown_hbm, sdown, 12)
-    for copy in first:
+    first[0].wait()
+    x = hid[...].astype(f32)
+    normed = (x * inv_rms(x, eps_norm) * attn_gain[...]).astype(bf16)
+    for b in range(blocks):
+        nbuf[b] = normed[:, b * depth : (b + 1) * depth]
+    for copy in first[1:]:
         copy.wait()
     pl.semaphore_wait(barrier, n - 1)
 
-    each_peer(lambda p: put(hid, gat.at[me], 0, p))
-    keep(hid, gat.at[me], 0)
-    own_rows = pl.ds(pl.multiple_of(me * rows, rows), rows)
-    in_owner = lambda c: (c * n) // in_tiles
-    stride = n // out_tiles
-    out_owner = lambda c: c * stride + stride - 1
-
-    def send_in(k, carry):
-        c = lax.rem(k + me, in_tiles)
-        cols_c = pl.ds(pl.multiple_of(c * LANES, LANES), LANES)
-        put_or_keep(w_in.at[:, cols_c], wq.at[own_rows, :], 1, in_owner(c))
-        return carry
-
-    lax.fori_loop(0, in_tiles, send_in, 0)
-
-    def send_out(k, carry):
-        c = lax.rem(k + me, out_tiles)
-        cols_c = pl.ds(pl.multiple_of(c * LANES, LANES), LANES)
-        put_or_keep(w_out.at[:, cols_c], wo.at[own_rows, :], 2, out_owner(c))
-        return carry
-
-    lax.fori_loop(0, out_tiles, send_out, 0)
-    my_in = (me * in_tiles + n - 1) // n
-    has_in = in_owner(my_in) == me
-    my_out = me // stride
-    has_out = lax.rem(me, stride) == stride - 1
+    each_peer(lambda p: put(nbuf.at[p // size], xin.at[me], 0, p))
+    keep(nbuf.at[me // size], xin.at[me], 0)
+    place = lax.rem(me, size)
+    own_rows = pl.ds(pl.multiple_of(place * rows, rows), rows)
+
+    def share(weights, block, dst, phase):
+        def part(q):
+            return weights.at[:, pl.ds(pl.multiple_of(q * block, block), block)]
+
+        def step(k, carry):
+            q = lax.rem(place + k, size)
+            put(part(q), dst.at[own_rows, :], phase, me - place + q)
+            return carry
+
+        lax.fori_loop(1, size, step, 0)
+        keep(part(place), dst.at[own_rows, :], phase)
+
+    share(w_in, in_block, wq, 1)
+    share(w_out, out_block, wo, 2)
 
     def stacked(buf, i):
         return jnp.concatenate(
             [buf[i * peers_step + k].astype(f32) for k in range(peers_step)], axis=0
-        )
-
-    wait_bytes(gat, recv_sem.at[0])
-
-    def norm_rows(i, carry):
-        x = stacked(gat, i)
-        at = pl.ds(pl.multiple_of(i * 16, 16), 16)
-        rows32[at, :] = x
-        rows16[at, :] = (x * inv_rms(x, eps_norm) * attn_gain[...]).astype(bf16)
-        return carry
-
-    lax.fori_loop(0, total // 16, norm_rows, 0)
-
-    @pl.when(has_in)
-    def _():
-        wait_bytes(wq, recv_sem.at[1])
-        sums = jnp.dot(rows16[...], wq[...], preferred_element_type=f32)
+        ).astype(bf16)
+
+    def stack(buf, dst):
+        def step(i, carry):
+            dst[pl.ds(pl.multiple_of(i * 16, 16), 16), :] = stacked(buf, i)
+            return carry
+
+        lax.fori_loop(0, total // 16, step, 0)
+
+    def project(buf, weights, sums, dst, phase):
+        stack(buf, xrows)
+        part = jnp.dot(xrows[...], weights[...], preferred_element_type=f32)
         for p in range(n):
-            csum[p] = sums[p * tok : (p + 1) * tok, :]
-        each_peer(lambda p: put(csum.at[p], proj.at[my_in], 3, p))
-        keep(csum.at[me], proj.at[my_in], 3)
+            sums[p] = part[p * tok : (p + 1) * tok, :]
+        each_peer(lambda p: put(sums.at[p], dst.at[me], phase, p))
+        keep(sums.at[me], dst.at[me], phase)
+
+    wait_bytes(xin, recv_sem.at[0])
+    wait_bytes(wq, recv_sem.at[1])
+    project(xin, wq, csum, proj, 3)
 
     row_id = lax.broadcasted_iota(jnp.int32, (tok, LANES), 0)
     position = jnp.zeros((tok, LANES), jnp.int32)
@@ -217,11 +212,20 @@
     load_keys.wait()
     load_values.wait()
     wait_bytes(proj, recv_sem.at[3])
+
+    def summed(buf, q):
+        whole = buf[q]
+        for b in range(1, blocks):
+            whole = whole + buf[b * size + q]
+        return whole
+
+    projected = jnp.concatenate([summed(proj, q) for q in range(size)], axis=1)
+    tiles = [projected[:, c * LANES : (c + 1) * LANES] for c in range(in_tiles)]
     turned = []
     for c in range(q_tiles + k_tiles):
-        x = proj[c]
+        x = tiles[c]
         turned.append((x * cosine + pltpu.roll(x, LANES // 2, 1) * sine).astype(bf16).astype(f32))
-    new_values = [proj[c].astype(bf16).astype(f32) for c in range(q_tiles + k_tiles, in_tiles)]
+    new_values = [tiles[c].astype(bf16).astype(f32) for c in range(q_tiles + k_tiles, in_tiles)]
     key_out[...] = jnp.concatenate(turned[q_tiles:], axis=1).astype(bf16)
     value_out[...] = jnp.concatenate(new_values, axis=1).astype(bf16)
     v_tiles = len(new_values) // KV_HEADS
@@ -287,39 +291,25 @@
             head = head * inv_rms(head, eps_head) * head_gain[...]
             heads += [head[g : g + 1] for g in range(group)]
         out_rows.append(jnp.concatenate(heads, axis=1))
-    abuf[...] = jnp.concatenate(out_rows, axis=0).astype(bf16)
-
-    def send_att(k, carry):
-        put_or_keep(abuf, att.at[me], 4, out_owner(lax.rem(k + my_out, out_tiles)))
-        return carry
-
-    lax.fori_loop(0, out_tiles, send_att, 0)
-
-    @pl.when(has_out)
-    def _():
-        wait_bytes(wo, recv_sem.at[2])
-        wait_bytes(att, recv_sem.at[4])
-
-        def stack_rows(i, carry):
-            rows16[pl.ds(pl.multiple_of(i * 16, 16), 16), :] = stacked(att, i).astype(bf16)
-            return carry
-
-        lax.fori_loop(0, total // 16, stack_rows, 0)
-        obuf[...] = jnp.dot(rows16[...], wo[...], preferred_element_type=f32).astype(bf16)
-        each_peer(lambda p: put(obuf, cols.at[my_out], 5, p, tile_sem.at[p]))
-        keep(obuf, cols.at[my_out], 5)
-
-    wait_bytes(cols, recv_sem.at[5])
-
-    def mix_rows(i, carry):
-        at = pl.ds(pl.multiple_of(i * 16, 16), 16)
-        added = jnp.concatenate([cols[c, at, :] for c in range(out_tiles)], axis=1)
-        x = (rows32[at, :] + added.astype(f32)).astype(bf16).astype(f32)
-        rows32[at, :] = x
-        rows16[at, :] = (x * inv_rms(x, eps_norm) * moe_gain[...]).astype(bf16)
-        return carry
-
-    lax.fori_loop(0, total // 16, mix_rows, 0)
+    attended = jnp.concatenate(out_rows, axis=0).astype(bf16)
+    for b in range(blocks):
+        abuf[b] = attended[:, b * depth : (b + 1) * depth]
+    each_peer(lambda p: put(abuf.at[p // size], att.at[me], 4, p))
+    keep(abuf.at[me // size], att.at[me], 4)
+
+    wait_bytes(wo, recv_sem.at[2])
+    wait_bytes(att, recv_sem.at[4])
+    project(att, wo, osum, oproj, 5)
+    wait_bytes(oproj, recv_sem.at[5])
+    attn_proj = jnp.concatenate([summed(oproj, q) for q in range(size)], axis=1)
+    after_mixer = hid[...].astype(f32) + attn_proj.astype(bf16).astype(f32)
+    after_mixer = after_mixer.astype(bf16).astype(f32)
+    moe_in = (after_mixer * inv_rms(after_mixer, eps_norm) * moe_gain[...]).astype(bf16)
+    mbuf[...] = moe_in
+    each_peer(lambda p: put(mbuf, gat.at[me], 6, p))
+    keep(mbuf, gat.at[me], 6)
+    wait_bytes(gat, recv_sem.at[6])
+    stack(gat, rows16)
     load_gate.wait()
     load_up.wait()
     load_down.wait()
@@ -344,24 +334,12 @@
         return carry
 
     lax.fori_loop(0, total // 16, split_rows, 0)
-    each_peer(lambda p: put(ebuf.at[p], back.at[me], 6, p))
-    keep(ebuf.at[me], back.at[me], 6)
+    each_peer(lambda p: put(ebuf.at[p], back.at[me], 7, p))
+    keep(ebuf.at[me], back.at[me], 7)
 
     load_sgate.wait()
     load_sup.wait()
     load_sdown.wait()
-    per_block = 8 // tok
-
-    def own(ref):
-        block = ref[pl.ds(pl.multiple_of(me // per_block * 8, 8), 8), :]
-        picked = block[:tok]
-        for k in range(1, per_block):
-            here = lax.rem(me, per_block) == k
-            picked = jnp.where(here, block[k * tok : (k + 1) * tok], picked)
-        return picked
-
-    after_mixer = own(rows32)
-    moe_in = (after_mixer * inv_rms(after_mixer, eps_norm) * moe_gain[...]).astype(bf16)
     shared_hidden = jnp.concatenate(
         [
             hide(moe_in, sgate, sup, slice(c * chunk, (c + 1) * chunk))
@@ -380,44 +358,33 @@
         ],
         axis=1,
     )
-    named = own(routing)
-    named_weight = own(route_weight)
-    expert_id = lax.broadcasted_iota(jnp.int32, (tok, n), 1)
-    table = jnp.zeros((tok, n), f32)
-    for k in range(named.shape[1]):
-        table = table + jnp.where(
-            expert_id == named[:, k : k + 1], named_weight[:, k : k + 1], 0.0
-        )
-    wait_bytes(back, recv_sem.at[6])
+    tokens, places = routing[...].astype(f32), route_weight[...]
+    column = lax.broadcasted_iota(jnp.int32, tokens.shape, 1)
+    expert_id = lax.broadcasted_iota(jnp.int32, (tokens.shape[0], n), 1).astype(f32)
+    lines = []
+    for s in range(tok):
+        here = column == me * tok + s
+        named = jnp.sum(jnp.where(here, tokens, 0.0), axis=1, keepdims=True)
+        weight = jnp.sum(jnp.where(here, places, 0.0), axis=1, keepdims=True)
+        chosen = jnp.where(expert_id == named, weight, 0.0)
+        lines.append(jnp.sum(chosen, axis=0, keepdims=True))
+    table = jnp.concatenate(lines, axis=0)
+    wait_bytes(back, recv_sem.at[7])
     routed = jnp.zeros((tok, width), f32)
     for e in range(n):
         routed = routed + table[:, e : e + 1] * back[e].astype(f32)
     out_ref[...] = (after_mixer + routed + shared_out).astype(bf16)
 
-    others = pl.ds(0, n - 1)
-    wait_bytes(gat.at[others], send_sem.at[0])
-    wait_bytes(back.at[others], send_sem.at[6])
-
-    def drain(mine, some, every, phase):
-        @pl.when(mine)
-        def _():
-            wait_bytes(some, send_sem.at[phase])
-
-        @pl.when(jnp.logical_not(mine))
-        def _():
-            wait_bytes(every, send_sem.at[phase])
-
-    drain(has_in, w_in.at[:, pl.ds(0, (in_tiles - 1) * LANES)], w_in, 1)
-    drain(has_out, w_out.at[:, pl.ds(0, (out_tiles - 1) * LANES)], w_out, 2)
-    drain(has_out, att.at[pl.ds(0, out_tiles - 1)], att.at[pl.ds(0, out_tiles)], 4)
-
-    @pl.when(has_in)
-    def _():
-        wait_bytes(csum.at[others], send_sem.at[3])
-
-    @pl.when(has_out)
-    def _():
-        each_peer(lambda p: wait_bytes(obuf, tile_sem.at[p]))
+    others, mates = pl.ds(0, n - 1), pl.ds(0, depth - rows)
+    sent = (xin.at[others], wq.at[mates], wo.at[mates], proj.at[others])
+    sent += (att.at[others], oproj.at[others], gat.at[others], back.at[others])
+    for phase, ref in enumerate(sent):
+        wait_bytes(ref, send_sem.at[phase])
+
+
+def hand_on(*refs):
+    for source, target in zip(refs[:3], refs[3:]):
+        target[...] = source[...]
 
 
 def on_device(
@@ -447,7 +414,9 @@
     total = n * tok
     rows = query_w.shape[0]
     in_width = query_w.shape[1] + key_w.shape[1] + value_w.shape[1]
-    in_tiles, out_tiles = in_width // LANES, width // LANES
+    size = math.gcd(in_width // LANES, width // LANES)
+    depth = size * rows
+    in_block, out_block = in_width // size, width // size
     half = HEAD_DIM // 2
     inverse = np.power(theta_base, -np.arange(half) / half).astype(np.float32)
     freqs = jnp.asarray(np.concatenate([inverse, inverse])[None, :])
@@ -455,13 +424,14 @@
     vmem = pl.BlockSpec(memory_space=pltpu.VMEM)
     hbm = pl.BlockSpec(memory_space=pl.ANY)
     like = lambda a: pltpu.VMEM(a.shape, a.dtype)
-    return pl.pallas_call(
-        functools.partial(layer_kernel, n),
-        out_shape=(
-            jax.ShapeDtypeStruct((tok, width), bf16),
+    shapes = (
+        jax.ShapeDtypeStruct((tok, width), bf16),
             jax.ShapeDtypeStruct((tok, key_w.shape[1]), bf16),
             jax.ShapeDtypeStruct((tok, value_w.shape[1]), bf16),
-        ),
+    )
+    results = pl.pallas_call(
+        functools.partial(layer_kernel, n),
+        out_shape=shapes,
         in_specs=[smem] * 2 + [hbm] * 13 + [vmem] * 6,
         out_specs=(vmem, vmem, vmem),
         scratch_shapes=[
@@ -476,25 +446,27 @@
             like(shared_gate),
             like(shared_up),
             like(shared_down),
-            pltpu.VMEM((n, tok, width), bf16),
-            pltpu.VMEM((n * rows, LANES), bf16),
-            pltpu.VMEM((n * out_w.shape[0], LANES), bf16),
-            pltpu.VMEM((total, width), f32),
-            pltpu.VMEM((total, width), bf16),
-            pltpu.VMEM((n, tok, LANES), f32),
-            pltpu.VMEM((in_tiles, tok, LANES), f32),
+            pltpu.VMEM((n // size, tok, depth), bf16),
+            pltpu.VMEM((n, tok, depth), bf16),
+            pltpu.VMEM((depth, in_block), bf16),
+            pltpu.VMEM((depth, out_block), bf16),
+            pltpu.VMEM((total, depth), bf16),
+            pltpu.VMEM((n, tok, in_block), f32),
+            pltpu.VMEM((n, tok, in_block), f32),
+            pltpu.VMEM((n // size, tok, depth), bf16),
+            pltpu.VMEM((n, tok, depth), bf16),
+            pltpu.VMEM((n, tok, out_block), f32),
+            pltpu.VMEM((n, tok, out_block), f32),
             pltpu.VMEM((tok, width), bf16),
             pltpu.VMEM((n, tok, width), bf16),
-            pltpu.VMEM((total, LANES), bf16),
-            pltpu.VMEM((out_tiles, total, LANES), bf16),
+            pltpu.VMEM((total, width), bf16),
             pltpu.VMEM((total, gate_w.shape[2]), bf16),
             pltpu.VMEM((total, width), f32),
             pltpu.VMEM((n, tok, width), bf16),
             pltpu.VMEM((n, tok, width), bf16),
             pltpu.SemaphoreType.DMA((13,)),
-            pltpu.SemaphoreType.DMA((7,)),
-            pltpu.SemaphoreType.DMA((7,)),
-            pltpu.SemaphoreType.DMA((n,)),
+            pltpu.SemaphoreType.DMA((8,)),
+            pltpu.SemaphoreType.DMA((8,)),
         ],
         compiler_params=pltpu.CompilerParams(
             collective_id=0, has_side_effects=True, vmem_limit_bytes=64000000
@@ -519,10 +491,17 @@
         head_gain[None, :],
         attn_gain[None, :],
         moe_gain[None, :],
-        routing,
-        route_weight,
+        routing.T,
+        route_weight.T,
         freqs,
     )
+    return pl.pallas_call(
+        hand_on,
+        out_shape=shapes,
+        in_specs=[vmem] * 3,
+        out_specs=(vmem,) * 3,
+        name="hand_on",
+    )(*results)
 
 
 def solution(mesh):

time: 65 us -> 50.5 us (0.78)
  Pallas kernels: 56.4 us -> 49 us
  local copies, waits for them, and re-layouts: 6.61 us -> 0 us
    pallas_call x1 -> x2, Pallas kernels: 56.4 us -> 49 us  [the longest x1 47.7 us: on_device(): pl.pallas_call(functools.partial(layer_kernel, n), out_shape=shapes, in_s...]
    unnamed x5 -> x0, local copies, waits for them, and re-layouts: 6.61 us -> none
where the time goes in v2:
time: 50.5 us; the launch traced here: 49.7 us
  Pallas kernels  49 us (97%)
  between operations  0.65 us (1%)
    pallas_call x1, Pallas kernels, on_device(): pl.pallas_call(functools.partial(layer_kernel, n), out_shape=shapes, in_s...  47.7 us
    pallas_call x1, Pallas kernels, on_device(): pl.pallas_call(hand_on, out_shape=shapes, in_specs=[vmem] * 3, out_specs=...  1.31 us

profile of v2, /device:TPU:0, one launch (start us, length us, event | category | flops | bytes accessed | tf_op | source)
XLA Modules:
  0.0 49.7 jit_solution(15878088329355664739)
XLA Ops:
  0.6 47.7 %decode_layer.1 = (bf16[2,2048]{1,0:T(2,128)(2,1)}, bf16[2,512]{1,0:T(2,128)(2,1)}, bf16[2,512]{1,0:T(2,128)(2,1)}) custom-call(s32[2]{0:T(128)} %lengths.1, f32[8]{0:T(128)} %lam.1, bf16[2,2048]{1,0:T(2,128)(2,1)} %hidden_hbm.1, bf16[2,1024,512]{2,1,0:T(8,128)(2,1)} %keys_hbm.1, bf16[2,1024,512]{2,1,0:T(8,128)(2,1)} %values_hbm.1, bf16[64,2048]{1,0:T(8,128)(2,1)} %qw_hbm.1, ...), custom_call_target="tpu_custom_call" | custom-call | tf_op jit(solution)/shard_map/decode_layer/pallas_call | solution.py:432
  48.4 1.3 %hand_on.1 = (bf16[2,2048]{1,0:T(2,128)(2,1)}, bf16[2,512]{1,0:T(2,128)(2,1)}, bf16[2,512]{1,0:T(2,128)(2,1)}) custom-call(bf16[2,2048]{1,0:T(2,128)(2,1)} %get-tuple-element.6.refs_0_, bf16[2,512]{1,0:T(2,128)(2,1)} %get-tuple-element.7.refs_1_, bf16[2,512]{1,0:T(2,128)(2,1)} %get-tuple-element.8.refs_2_), custom_call_target="tpu_custom_call" | custom-call | tf_op jit(solution)/shard_map/hand_on/pallas_call | solution.py:498

commit v3 on v2

--- a/solution.py
+++ b/solution.py
@@ -88,6 +88,7 @@
     local_sem,
     send_sem,
     recv_sem,
+    row_sem,
 ):
     me = lax.axis_index("ep")
     tok, width = hid.shape
@@ -306,9 +307,49 @@
     after_mixer = after_mixer.astype(bf16).astype(f32)
     moe_in = (after_mixer * inv_rms(after_mixer, eps_norm) * moe_gain[...]).astype(bf16)
     mbuf[...] = moe_in
-    each_peer(lambda p: put(mbuf, gat.at[me], 6, p))
-    keep(mbuf, gat.at[me], 6)
-    wait_bytes(gat, recv_sem.at[6])
+    mate = me + 1 - 2 * lax.rem(me, 2)
+    chips = n // 2
+
+    def to_chip(k, carry):
+        chip = lax.rem(me // 2 + chips // 2 + k, chips)
+        p = chip * 2 + lax.rem(me, 2)
+
+        @pl.when(p != me)
+        def _():
+            pltpu.make_async_remote_copy(
+                src_ref=mbuf,
+                dst_ref=gat.at[me],
+                send_sem=send_sem.at[6],
+                recv_sem=row_sem.at[me],
+                device_id=(p,),
+                device_id_type=MESH,
+            ).start()
+
+        return carry
+
+    def send_on(k, carry):
+        chip = lax.rem(me // 2 + k, chips)
+        p = chip * 2 + lax.rem(me, 2)
+        wait_bytes(gat.at[p], row_sem.at[p])
+        pass_on(gat.at[p], p)
+        return carry
+
+    def pass_on(src, p):
+        pltpu.make_async_remote_copy(
+            src_ref=src,
+            dst_ref=gat.at[p],
+            send_sem=send_sem.at[8],
+            recv_sem=recv_sem.at[6],
+            device_id=(mate,),
+            device_id_type=MESH,
+        ).start()
+
+    lax.fori_loop(0, chips, to_chip, 0)
+    pass_on(mbuf, me)
+    own_copy = load(mbuf, gat.at[me], 13)
+    lax.fori_loop(1, chips, send_on, 0)
+    own_copy.wait()
+    wait_bytes(gat.at[pl.ds(0, chips)], recv_sem.at[6])
     stack(gat, rows16)
     load_gate.wait()
     load_up.wait()
@@ -377,7 +418,8 @@
 
     others, mates = pl.ds(0, n - 1), pl.ds(0, depth - rows)
     sent = (xin.at[others], wq.at[mates], wo.at[mates], proj.at[others])
-    sent += (att.at[others], oproj.at[others], gat.at[others], back.at[others])
+    sent += (att.at[others], oproj.at[others], gat.at[pl.ds(0, n // 2 - 1)], back.at[others])
+    sent += (gat.at[pl.ds(0, n // 2)],)
     for phase, ref in enumerate(sent):
         wait_bytes(ref, send_sem.at[phase])
 
@@ -464,9 +506,10 @@
             pltpu.VMEM((total, width), f32),
             pltpu.VMEM((n, tok, width), bf16),
             pltpu.VMEM((n, tok, width), bf16),
-            pltpu.SemaphoreType.DMA((13,)),
+            pltpu.SemaphoreType.DMA((14,)),
+            pltpu.SemaphoreType.DMA((9,)),
             pltpu.SemaphoreType.DMA((8,)),
-            pltpu.SemaphoreType.DMA((8,)),
+            pltpu.SemaphoreType.DMA((n,)),
         ],
         compiler_params=pltpu.CompilerParams(
             collective_id=0, has_side_effects=True, vmem_limit_bytes=64000000

time: 50.5 us -> 49.4 us (0.978); the launches traced: 49.7 us -> 49.2 us
  no operation moved by 1% of the time
where the time goes in v3:
time: 49.4 us; the launch traced here: 49.2 us
  Pallas kernels  48.6 us (98%)
  between operations  0.65 us (1%)
    pallas_call x1, Pallas kernels, on_device(): pl.pallas_call(functools.partial(layer_kernel, n), out_shape=shapes, in_s...  47.2 us
    pallas_call x1, Pallas kernels, on_device(): pl.pallas_call(hand_on, out_shape=shapes, in_specs=[vmem] * 3, out_specs=...  1.31 us

profile of v3, /device:TPU:0, one launch (start us, length us, event | category | flops | bytes accessed | tf_op | source)
XLA Modules:
  0.0 49.2 jit_solution(10538695998358358460)
XLA Ops:
  0.6 47.2 %decode_layer.1 = (bf16[2,2048]{1,0:T(2,128)(2,1)}, bf16[2,512]{1,0:T(2,128)(2,1)}, bf16[2,512]{1,0:T(2,128)(2,1)}) custom-call(s32[2]{0:T(128)} %lengths.1, f32[8]{0:T(128)} %lam.1, bf16[2,2048]{1,0:T(2,128)(2,1)} %hidden_hbm.1, bf16[2,1024,512]{2,1,0:T(8,128)(2,1)} %keys_hbm.1, bf16[2,1024,512]{2,1,0:T(8,128)(2,1)} %values_hbm.1, bf16[64,2048]{1,0:T(8,128)(2,1)} %qw_hbm.1, ...), custom_call_target="tpu_custom_call" | custom-call | tf_op jit(solution)/shard_map/decode_layer/pallas_call | solution.py:474
  47.9 1.3 %hand_on.1 = (bf16[2,2048]{1,0:T(2,128)(2,1)}, bf16[2,512]{1,0:T(2,128)(2,1)}, bf16[2,512]{1,0:T(2,128)(2,1)}) custom-call(bf16[2,2048]{1,0:T(2,128)(2,1)} %get-tuple-element.6.refs_0_, bf16[2,512]{1,0:T(2,128)(2,1)} %get-tuple-element.7.refs_1_, bf16[2,512]{1,0:T(2,128)(2,1)} %get-tuple-element.8.refs_2_), custom_call_target="tpu_custom_call" | custom-call | tf_op jit(solution)/shard_map/hand_on/pallas_call | solution.py:541
